TPU v7x, 32 devices: a whole 2x2x4 slice. The times are simulated.
32 devices in a mesh: grp: 2 (over y), sp: 4 (over z), dp: 4 (over x, core).
Axes of the slice: x: 2, y: 2, z: 4, core: 2. Of those that a mesh axis runs over, the one named last changes fastest.
Arguments:
- tokens: bfloat16 [8, 1536, 2048], P(('grp', 'dp'), 'sp'), parts along dimension 0, may hold values from -6 to 6
- w_value: bfloat16 [2048, 1024], P('dp', 'sp'), may hold values from -0.125 to 0.125
- w_gate: bfloat16 [2048, 1024], P('dp', 'sp'), may hold values from -0.125 to 0.125
- conv_weight: bfloat16 [31, 1024], replicated, may hold values from -20 to 20
- norm_gain: float32 [1024], replicated, may hold values from 0.1 to 1.9
- norm_bias: float32 [1024], replicated, may hold values from -3 to 3
- w_out: bfloat16 [1024, 2048], P('sp', 'dp'), may hold values from -0.1875 to 0.1875
Outputs:
- mixed: bfloat16 [8, 1536, 2048], P(('grp', 'dp'), 'sp'), parts along dimension 0
There are 2 independent parts, one for each index of `grp`. A program takes and returns all parts, laid end to end along the dimension named above; an argument that names none is the same for every part. Nothing has to cross between parts.
All inputs are finite; a program needn't handle non-finite values.
Results may differ from a plain program's by a relative error of at most 0.012.
Values may be sent and summed in bfloat16 or wider, within the bound.
A program may use at most 64 MiB of HBM per device.

v0:
```python
import jax
import jax.numpy as jnp
from jax import lax
from jax.sharding import PartitionSpec as P

EPS = 1e-05


def passed_along(array, axis, by):
    peers = lax.axis_size(axis)
    pairs = [(i, i + by) for i in range(peers) if 0 <= i + by < peers]
    return lax.ppermute(array, axis, pairs)


def per_device(tokens, w_value, w_gate, conv_weight, norm_gain, norm_bias, w_out):
    pieces = (
        lax.all_gather(w_value, "sp", axis=1, tiled=True),
        lax.all_gather(w_gate, "sp", axis=1, tiled=True),
        lax.all_gather(w_out, "sp", axis=0, tiled=True),
    )
    full_value, full_gate, full_out = (
        lax.all_gather(pieces[0], "dp", axis=0, tiled=True),
        lax.all_gather(pieces[1], "dp", axis=0, tiled=True),
        lax.all_gather(pieces[2], "dp", axis=1, tiled=True),
    )
    rows = tokens[0]
    kernel_width = conv_weight.shape[0]
    channels = norm_gain.shape[0]
    value = jnp.dot(rows, full_value, preferred_element_type=jnp.float32)
    gate = jnp.dot(rows, full_gate, preferred_element_type=jnp.float32)
    glu = (value * jax.nn.sigmoid(gate)).astype(jnp.bfloat16)
    earlier = passed_along(glu[rows.shape[0] - (kernel_width - 1) :], "sp", 1)
    extended = jnp.concatenate([earlier, glu], axis=0)
    kernel = conv_weight[::-1][:, None, :]
    conv = lax.conv_general_dilated(
        extended[None],
        kernel,
        (1,),
        [(0, 0)],
        dimension_numbers=("NWC", "WIO", "NWC"),
        feature_group_count=channels,
        preferred_element_type=jnp.float32,
    )[0].astype(jnp.bfloat16)
    conv_f = conv.astype(jnp.float32)
    mean = jnp.mean(conv_f, axis=1, keepdims=True)
    meansq = jnp.mean(conv_f * conv_f, axis=1, keepdims=True)
    scaled = (conv_f - mean) * lax.rsqrt(meansq - mean * mean + EPS) * norm_gain + norm_bias
    normed = jax.nn.silu(scaled).astype(jnp.bfloat16)
    mixed = jnp.dot(normed, full_out, preferred_element_type=jnp.float32)
    return mixed.astype(jnp.bfloat16)[None]


def solution(mesh):
    placed = (
        P(("grp", "dp"), "sp", None),
        P("dp", "sp"),
        P("dp", "sp"),
        P(),
        P(),
        P(),
        P("sp", "dp"),
    )
    return jax.shard_map(
        per_device,
        mesh=mesh,
        in_specs=placed,
        out_specs=P(("grp", "dp"), "sp", None),
        check_vma=False,
    )
```

profile of v0, /device:TPU:1, one launch (start us, length us, event | category | flops | bytes accessed | tf_op | source)
XLA Modules:
  0.0 218.5 jit_solution(2104043938752544251)
XLA Ops:
  6.5 0.0 copy-start
  6.5 0.0 all-gather.11.cloned.1.call-start
  6.5 0.7 all-gather.11.cloned.1.call-update
  7.3 0.0 all-gather.7.cloned.1.call-start
  7.3 0.7 all-gather.7.cloned.1.call-update
  8.0 0.0 all-gather.15.cloned.1.call-start
  8.1 0.7 all-gather.15.cloned.1.call-update
  8.7 0.0 all-gather.13.cloned.1.call-start
  8.8 30.8 %all-gather.11.cloned.1.call-done = bf16[512,1024]{1,0:T(8,128)(2,1)} async-done(((bf16[512,256]{1,0:T(8,128)(2,1)}), bf16[512,1024]{1,0:T(8,128)(2,1)}) %all-gather.11.cloned.1.call-update) | async-done | bytes 1048592 | tf_op jit(solution)/shard_map/all_gather | solution.py:18
  39.6 0.0 all-gather.13.cloned.1.call-update
  39.6 0.0 all-gather.9.cloned.1.call-start
  39.6 29.8 %all-gather.7.cloned.1.call-done = bf16[512,1024]{1,0:T(8,128)(2,1)} async-done(((bf16[512,256]{1,0:T(8,128)(2,1)}), bf16[512,1024]{1,0:T(8,128)(2,1)}) %all-gather.7.cloned.1.call-update) | async-done | bytes 1048592 | tf_op jit(solution)/shard_map/all_gather | solution.py:17
  69.4 0.0 all-gather.9.cloned.1.call-update
  69.4 0.0 all-gather.17.cloned.1.call-start
  69.5 28.7 %all-gather.15.cloned.1.call-done = bf16[1024,512]{1,0:T(8,128)(2,1)} async-done(((bf16[256,512]{1,0:T(8,128)(2,1)}), bf16[1024,512]{1,0:T(8,128)(2,1)}) %all-gather.15.cloned.1.call-update) | async-done | bytes 1048592 | tf_op jit(solution)/shard_map/all_gather | solution.py:19
  98.2 0.0 all-gather.17.cloned.1.call-update
  98.2 36.1 %all-gather.13.cloned.1.call-done = bf16[2048,1024]{1,0:T(8,128)(2,1)} async-done(((bf16[512,1024]{1,0:T(8,128)(2,1)}), bf16[2048,1024]{1,0:T(8,128)(2,1)}) %all-gather.13.cloned.1.call-update) | async-done | bytes 4194320 | tf_op jit(solution)/shard_map/all_gather | solution.py:23
  134.3 0.0 copy-done
  134.3 5.1 %fusion.6 = f32[384,1024]{1,0:T(8,128)} fusion(bf16[2048,1024]{1,0:T(8,128)(2,1)} %all-gather.13.cloned.1.call-done, bf16[1,384,2048]{2,1,0:T(8,128)(2,1)S(1)} %copy-done), kind=kOutput, calls=%fused_computation.11 | convolution fusion | flops 1610612736 | bytes 7340032 | tf_op jit(solution)/shard_map/dot_general | solution.py:30
  139.4 0.0 copy-start.1
  139.4 30.8 %all-gather.9.cloned.1.call-done = bf16[2048,1024]{1,0:T(8,128)(2,1)} async-done(((bf16[512,1024]{1,0:T(8,128)(2,1)}), bf16[2048,1024]{1,0:T(8,128)(2,1)}) %all-gather.9.cloned.1.call-update) | async-done | bytes 4194320 | tf_op jit(solution)/shard_map/all_gather | solution.py:22
  170.2 4.5 %multiply_convert_fusion.1 = bf16[384,1024]{1,0:T(8,128)(2,1)S(1)} fusion(f32[384,1024]{1,0:T(8,128)} %fusion.6, bf16[2048,1024]{1,0:T(8,128)(2,1)} %all-gather.9.cloned.1.call-done, bf16[1,384,2048]{2,1,0:T(8,128)(2,1)S(1)} %copy-done), kind=kOutput, calls=%fused_computation.16 | convolution fusion | flops 1612578816 | bytes 8126464 | tf_op jit(solution)/shard_map/dot_general | solution.py:29
  174.8 3.1 %collective-permute-start = (bf16[30,1024]{1,0:T(8,128)(2,1)S(1)}, bf16[30,1024]{1,0:T(8,128)(2,1)S(1)}, u32[]{:S(2)}, u32[]{:S(2)}) collective-permute-start(bf16[30,1024]{1,0:T(8,128)(2,1)S(1)} %slice.6), channel_id=1, source_target_pairs={{0,4},{4,8},{8,12},{1,5},{5,9},{9,13},{2,6},{6,10},{10,14},{3,7},{... | collective-permute-start | bytes 184328 | tf_op jit(solution)/shard_map/ppermute | solution.py:12
  177.9 0.0 copy-done.1
  177.9 0.3 rev.3
  178.2 1.0 collective-permute-done
  179.2 0.2 maximum_bitcast_fusion
  179.4 0.1 pad
  179.5 0.2 reshape.24
  179.6 0.0 copy-start.4
  179.7 0.5 copy.13
  180.1 0.1 slice.7
  180.3 0.1 copy-done.4
  180.3 3.8 %fusion.21 = f32[8,52,1024]{2,0,1:T(8,128)S(1)} fusion(bf16[1,7,30,1024]{3,1,2,0:T(8,128)(2,1)S(1)} %slice.7, bf16[1,8,52,1024]{3,1,2,0:T(8,128)(2,1)S(1)} %copy.13, pred[8,52]{0,1:T(8,128)(4,1)S(1)} %copy-done.4, bf16[31,1,1024]{2,0,1:T(8,128)(2,1)S(1)} %bitcast.36), kind=kOutput, calls=%fused_computation.24 | convolution fusion | flops 31719424 | bytes 3049888 | tf_op jit(solution)/shard_map/conv_general_dilated | solution.py:35
  184.1 2.2 %copy.15 = f32[8,52,1024]{2,1,0:T(8,128)} copy(f32[8,52,1024]{2,0,1:T(8,128)S(1)} %fusion.21) | data formatting | bytes 3407872 | tf_op jit(solution)/shard_map/convert_element_type | solution.py:44
  186.4 1.6 reshape.28
  187.9 0.0 copy-start.2
  187.9 0.0 copy-start.3
  188.0 0.2 slice_reduce_fusion
  188.1 0.2 fusion.5
  188.3 17.8 %all-gather.17.cloned.1.call-done = bf16[1024,2048]{1,0:T(8,128)(2,1)} async-done(((bf16[1024,512]{1,0:T(8,128)(2,1)}), bf16[1024,2048]{1,0:T(8,128)(2,1)}) %all-gather.17.cloned.1.call-update) | async-done | bytes 4194320 | tf_op jit(solution)/shard_map/all_gather | solution.py:24
  206.1 0.0 copy-done.2
  206.1 0.0 copy-done.3
  206.1 5.5 %fusion.1 = bf16[1,384,2048]{2,1,0:T(8,128)(2,1)} fusion(bf16[1024,2048]{1,0:T(8,128)(2,1)} %all-gather.17.cloned.1.call-done, f32[1,416,1024]{2,1,0:T(8,128)S(1)} %reshape.28, f32[1024]{0:T(1024)S(1)} %copy-done.2, f32[1024]{0:T(1024)S(1)} %copy-done.3, f32[384]{0:T(512)S(1)} %get-tuple-element.6, f32[384]{0:T(512)S(1)} %get-tuple-element.5), kind=kOutput, calls=%fused_computation.3 | convolution fusion | flops 1614938112 | bytes 7352320 | tf_op jit(solution)/shard_map/dot_general | solution.py:49
  (2 shorter events, 0.0 us)
Async XLA Ops:
  6.5 127.8 %copy-start = (bf16[1,384,2048]{2,1,0:T(8,128)(2,1)S(1)}, bf16[1,384,2048]{2,1,0:T(8,128)(2,1)}, u32[]{:S(2)}) copy-start(bf16[1,384,2048]{2,1,0:T(8,128)(2,1)} %param.7) | copy-start | bytes 4718596
  6.5 33.0 %all-gather.11.cloned.1.call-start = ((), (), s32[]{:S(2)}) async-start(), calls=%async_computation.2 | async-start | bytes 1310720 | tf_op jit(solution)/shard_map/all_gather | solution.py:18
  7.3 62.1 %all-gather.7.cloned.1.call-start = ((), (), s32[]{:S(2)}) async-start(), calls=%async_computation | async-start | bytes 1310720 | tf_op jit(solution)/shard_map/all_gather | solution.py:17
  8.0 90.2 %all-gather.15.cloned.1.call-start = ((), (), s32[]{:S(2)}) async-start(), calls=%async_computation.4 | async-start | bytes 1310720 | tf_op jit(solution)/shard_map/all_gather | solution.py:19
  8.7 125.6 %all-gather.13.cloned.1.call-start = ((), (), s32[]{:S(2)}) async-start(), calls=%async_computation.3 | async-start | bytes 5242880 | tf_op jit(solution)/shard_map/all_gather | solution.py:23
  39.6 130.6 %all-gather.9.cloned.1.call-start = ((), (), s32[]{:S(2)}) async-start(), calls=%async_computation.1 | async-start | bytes 5242880 | tf_op jit(solution)/shard_map/all_gather | solution.py:22
  69.4 136.7 %all-gather.17.cloned.1.call-start = ((), (), s32[]{:S(2)}) async-start(), calls=%async_computation.5 | async-start | bytes 5242880 | tf_op jit(solution)/shard_map/all_gather | solution.py:24
  139.4 38.5 %copy-start.1 = (bf16[31,1024]{1,0:T(8,128)(2,1)S(1)}, bf16[31,1024]{1,0:T(8,128)(2,1)}, u32[]{:S(2)}) copy-start(bf16[31,1024]{1,0:T(8,128)(2,1)} %param.10) | copy-start | bytes 190468
  174.8 4.4 %collective-permute-start = (bf16[30,1024]{1,0:T(8,128)(2,1)S(1)}, bf16[30,1024]{1,0:T(8,128)(2,1)S(1)}, u32[]{:S(2)}, u32[]{:S(2)}) collective-permute-start(bf16[30,1024]{1,0:T(8,128)(2,1)S(1)} %slice.6), channel_id=1, source_target_pairs={{0,4},{4,8},{8,12},{1,5},{5,9},{9,13},{2,6},{6,10},{10,14},{3,7},{... | collective-permute-start | bytes 184328 | tf_op jit(solution)/shard_map/ppermute | solution.py:12
  179.6 0.7 copy-start.4
  187.9 18.2 %copy-start.2 = (f32[1024]{0:T(1024)S(1)}, f32[1024]{0:T(1024)}, u32[]{:S(2)}) copy-start(f32[1024]{0:T(1024)} %param.12) | copy-start | bytes 12292
  187.9 18.2 %copy-start.3 = (f32[1024]{0:T(1024)S(1)}, f32[1024]{0:T(1024)}, u32[]{:S(2)}) copy-start(f32[1024]{0:T(1024)} %param.11) | copy-start | bytes 12292
Sparse Core Ops, SparseCore 0:
  8.9 30.6 all-gather.10
  41.1 28.2 all-gather.6
  71.0 27.1 all-gather.14
  99.6 34.6 all-gather.12
  135.7 34.4 all-gather.8
  171.6 34.4 all-gather.16
where the time goes:
time: 219 us; the launch traced here: 218 us
  waiting for transfers between devices  177 us (81%)
  matrix products  18.9 us (9%)
  between operations  13.6 us (6%)
  local copies, waits for them, and re-layouts  5 us (2%)
  starting transfers between devices  3.3 us (2%)
    all_gather x1, waiting for transfers between devices, per_device(): lax.all_gather(pieces[1], 'dp', axis=0, tiled=True)  36.1 us
    all_gather x1, waiting for transfers between devices, per_device(): lax.all_gather(w_gate, 'sp', axis=1, tiled=True)  30.8 us
    all_gather x1, waiting for transfers between devices, per_device(): lax.all_gather(pieces[0], 'dp', axis=0, tiled=True)  30.8 us
    all_gather x1, waiting for transfers between devices, per_device(): lax.all_gather(w_value, 'sp', axis=1, tiled=True)  29.8 us
    all_gather x1, waiting for transfers between devices, per_device(): lax.all_gather(w_out, 'sp', axis=0, tiled=True)  28.7 us
    all_gather x1, waiting for transfers between devices, per_device(): lax.all_gather(pieces[2], 'dp', axis=1, tiled=True)  17.8 us
    dot_general x1, matrix products, per_device(): mixed = jnp.dot(normed, full_out, preferred_element_type=jnp.float32)  5.51 us
    dot_general x1, matrix products, per_device(): gate = jnp.dot(rows, full_gate, preferred_element_type=jnp.float32)  5.12 us
  transfers between devices with their start and end apart: 7, of which 7 were waited for; matrix products, arithmetic and copies ran while one was open for 9% of the time, Pallas kernels for 0%

commit v1 on v0

--- a/solution.py
+++ b/solution.py
@@ -1,9 +1,312 @@
+import functools
 import jax
 import jax.numpy as jnp
 from jax import lax
+from jax.experimental import pallas as pl
+from jax.experimental.pallas import tpu as pltpu
 from jax.sharding import PartitionSpec as P
 
 EPS = 1e-05
+LANES = 128
+PACK = 16
+MESH = pl.DeviceIdType.MESH
+
+
+def round_up(n, to):
+    return -(-n // to) * to
+
+
+def fused_kernel(
+    n_sp,
+    x_ref,
+    wv_ref,
+    wg_ref,
+    wo_ref,
+    cw_ref,
+    gain_ref,
+    bias_ref,
+    out_ref,
+    bv,
+    bg,
+    bo,
+    xt,
+    value,
+    ext,
+    taps,
+    conv,
+    normed,
+    acc,
+    stage,
+    z_send,
+    z_recv,
+    x_send,
+    x_recv,
+    y_send,
+    y_recv,
+    c_send,
+    c_recv,
+    h_sem,
+    l_sem,
+    o_sem,
+):
+    z = lax.axis_index("sp")
+    y = lax.axis_index("grp")
+    dp = lax.axis_index("dp")
+    core = lax.rem(dp, 2)
+    twin = dp + 1 - 2 * core
+    across = lax.rem(dp + 2, 4)
+    n_dp = bo.shape[1]
+    rows = x_ref.shape[0]
+    total_rows = xt.shape[0]
+    lead = total_rows - rows
+    n_taps = cw_ref.shape[0]
+    chunk = bv.shape[2]
+    per_chunk = chunk // LANES
+    groups = ext.shape[0]
+    own = (wv_ref, wg_ref, wo_ref)
+    bufs = (bv, bg, bo)
+
+    def at_z(k):
+        return lax.rem(z + k, n_sp)
+
+    def span(m):
+        size = own[m].shape[0]
+        only = round_up(size * 5 // 16, PACK)
+        return size, only, size - only
+
+    def region(m, zz, dd, start, size):
+        if m == 2:
+            return bo.at[zz, dd, pl.ds(start, size), :]
+        depth = own[m].shape[0]
+        return bufs[m].at[zz, pl.ds(pl.multiple_of(dd * depth + start, PACK), size), :]
+
+    def share(m):
+        size, only, most = span(m)
+        return pl.multiple_of(y * only, PACK), most
+
+    def gives(m):
+        size, only, most = span(m)
+        return pl.multiple_of(y * most, PACK), only
+
+    def lacks(m):
+        size, only, most = span(m)
+        return pl.multiple_of((1 - y) * most, PACK), only
+
+    started = []
+
+    def remote(src, dst, send, recv, where):
+        return pltpu.make_async_remote_copy(
+            src_ref=src, dst_ref=dst, send_sem=send, recv_sem=recv, device_id=where, device_id_type=MESH
+        )
+
+    def send(*a):
+        copy = remote(*a)
+        copy.start()
+        started.append(copy)
+
+    own_copies = [
+        pltpu.make_async_copy(own[m], region(m, z, dp, 0, own[m].shape[0]), l_sem.at[m]) for m in range(3)
+    ]
+    x_copy = pltpu.make_async_copy(x_ref, xt.at[pl.ds(lead, rows), :], l_sem.at[3])
+    for c in (own_copies[0], x_copy, own_copies[1], own_copies[2]):
+        c.start()
+
+    barrier = pltpu.get_barrier_semaphore()
+    peers = [{"sp": at_z(k)} for k in range(1, n_sp)] + [{"dp": across}, {"grp": 1 - y}, {"dp": twin}]
+    for peer in peers:
+        pl.semaphore_signal(barrier, inc=1, device_id=peer, device_id_type=MESH)
+    pl.semaphore_wait(barrier, len(peers))
+
+    def own_share(m):
+        start, size = share(m)
+        return own[m].at[pl.ds(start, size), :], region(m, z, dp, start, size)
+
+    def send_z(m, k):
+        src, dst = own_share(m)
+        send(src, dst, z_send.at[m, k - 1], z_recv.at[m, k - 1], {"sp": lax.rem(z + n_sp - k, n_sp)})
+
+    def send_halo():
+        send(
+            x_ref.at[pl.ds(rows - lead, lead), :], xt.at[pl.ds(0, lead), :], h_sem.at[0], h_sem.at[1], {"sp": at_z(1)}
+        )
+
+    for m in range(3):
+        src, dst = own_share(m)
+        send_z(m, 1)
+        send(src, dst, x_send.at[m, 0], x_recv.at[m, 0], {"dp": across})
+        if m == 0:
+            send_halo()
+        for k in range(2, n_sp):
+            send_z(m, k)
+        whole = region(m, z, dp, 0, own[m].shape[0])
+        send(own[m], whole, c_send.at[m, 0, 0], c_recv.at[m, 0, 0], {"dp": twin})
+
+    for j in range(groups):
+        taps[j, 0:n_taps, :] = cw_ref[:, j * LANES : (j + 1) * LANES].astype(jnp.float32)
+
+    def forward_y(m, k, side, dd):
+        start, size = gives(m)
+        part = region(m, at_z(k), dd, start, size)
+        send(part, part, y_send.at[m, k, side], y_recv.at[m, k, side], {"grp": 1 - y})
+
+    def step_zx(m, k):
+        start, size = share(m)
+        if k > 0:
+            part = region(m, at_z(k), dp, start, size)
+            remote(part, part, z_send.at[m, k - 1], z_recv.at[m, k - 1], {"sp": z}).wait_recv()
+            send(part, part, x_send.at[m, k], x_recv.at[m, k], {"dp": across})
+            forward_y(m, k, 0, dp)
+        part = region(m, at_z(k), across, start, size)
+        remote(part, part, x_send.at[m, k], x_recv.at[m, k], {"dp": across}).wait_recv()
+        forward_y(m, k, 1, across)
+
+    def step_y(m, k):
+        start, size = lacks(m)
+        for side, dd in ((0, dp), (1, across)):
+            if k == 0 and side == 0:
+                continue
+            part = region(m, at_z(k), dd, start, size)
+            remote(part, part, y_send.at[m, k, side], y_recv.at[m, k, side], {"grp": 1 - y}).wait_recv()
+            whole = region(m, at_z(k), dd, 0, own[m].shape[0])
+            send(whole, whole, c_send.at[m, k, side], c_recv.at[m, k, side], {"dp": twin})
+
+    def conv_group(j):
+        tile = rows // 4
+        for r in range(4):
+            base = lead + r * tile
+            total = jnp.zeros((tile, LANES), jnp.float32)
+            for tap in range(n_taps):
+                total = total + taps[j, tap : tap + 1, :] * ext[j, base - tap : base - tap + tile, :]
+            conv[j, r * tile : (r + 1) * tile, :] = total.astype(jnp.bfloat16)
+
+    def step_norm():
+        tile = 2 * PACK
+        channels = groups * LANES
+
+        @pl.loop(0, rows // tile)
+        def _(i):
+            at = pl.ds(pl.multiple_of(i * tile, tile), tile)
+            parts = [conv[j, at, :].astype(jnp.float32) for j in range(groups)]
+            plain = functools.reduce(jnp.add, parts)
+            square = functools.reduce(jnp.add, [p * p for p in parts])
+            mean = jnp.sum(plain, axis=1, keepdims=True) * (1.0 / channels)
+            meansq = jnp.sum(square, axis=1, keepdims=True) * (1.0 / channels)
+            scale = lax.rsqrt(meansq - mean * mean + EPS)
+            for j in range(groups):
+                cols = slice(j * LANES, (j + 1) * LANES)
+                v = (parts[j] - mean) * scale * gain_ref[:, cols] + bias_ref[:, cols]
+                v = v / (1.0 + jnp.exp(-v))
+                q, h = divmod(j, per_chunk)
+                normed[q, at, h * LANES : (h + 1) * LANES] = v.astype(jnp.bfloat16)
+
+    out_copies = []
+
+    def step_use(m, k):
+        zk = at_z(k)
+        for side, dd in ((0, lax.rem(dp + 1 - 2 * core, n_dp)), (1, lax.rem(across + 1 - 2 * core, n_dp))):
+            whole = region(m, zk, dd, 0, own[m].shape[0])
+            remote(whole, whole, c_send.at[m, k, side], c_recv.at[m, k, side], {"dp": twin}).wait_recv()
+        if k == 0:
+            own_copies[m].wait()
+            if m == 0:
+                x_copy.wait()
+                tail = xt.at[pl.ds(0, lead), :]
+                remote(tail, tail, h_sem.at[0], h_sem.at[1], {"sp": z}).wait_recv()
+        if m == 0:
+            value[zk] = jnp.dot(xt[...], bv[zk], preferred_element_type=jnp.float32)
+        elif m == 1:
+            gate = jnp.dot(xt[...], bg[zk], preferred_element_type=jnp.float32)
+            glu = (value[zk] * jax.nn.sigmoid(gate)).astype(jnp.bfloat16).astype(jnp.float32)
+            before = jnp.where(z == 0, 0.0, 1.0)
+            for h in range(per_chunk):
+                cols = slice(h * LANES, (h + 1) * LANES)
+                ext[zk * per_chunk + h, 0:lead, :] = glu[:lead, cols] * before
+                ext[zk * per_chunk + h, lead:, :] = glu[lead:, cols]
+
+            @pl.loop(0, per_chunk)
+            def _(h):
+                conv_group(zk * per_chunk + h)
+
+            if k == n_sp - 1:
+                step_norm()
+        else:
+            for d in range(n_dp):
+                part = jnp.dot(normed[zk], bo[zk, d], preferred_element_type=jnp.float32)
+                if k > 0:
+                    part = part + acc[d]
+                if k < n_sp - 1:
+                    acc[d] = part
+                else:
+                    width = bo.shape[3]
+                    stage[d] = part.astype(jnp.bfloat16)
+                    copy = pltpu.make_async_copy(
+                        stage.at[d], out_ref.at[:, d * width : (d + 1) * width], o_sem.at[d]
+                    )
+                    copy.start()
+                    out_copies.append(copy)
+
+    order = [(m, k) for m in range(3) for k in range(n_sp)]
+    for t in range(len(order) + 2):
+        if t < len(order):
+            step_zx(*order[t])
+        if 0 <= t - 1 < len(order):
+            step_y(*order[t - 1])
+        if t >= 2:
+            step_use(*order[t - 2])
+
+    for copy in started:
+        copy.wait_send()
+    for copy in out_copies:
+        copy.wait()
+
+
+def fused(n_sp, tokens, w_value, w_gate, conv_weight, norm_gain, norm_bias, w_out):
+    rows, model = tokens.shape[1:]
+    depth, chunk = w_value.shape
+    deep, width = w_out.shape
+    n_dp = model // depth
+    n_taps, channels = conv_weight.shape
+    lead = round_up(n_taps - 1, 2 * PACK)
+    groups = channels // LANES
+    total = rows + lead
+    bf16, f32 = jnp.bfloat16, jnp.float32
+    dma = pltpu.SemaphoreType.DMA
+    anywhere = pl.BlockSpec(memory_space=pl.ANY)
+    vmem = pl.BlockSpec(memory_space=pltpu.VMEM)
+    out = pl.pallas_call(
+        functools.partial(fused_kernel, n_sp),
+        out_shape=jax.ShapeDtypeStruct((rows, model), bf16),
+        in_specs=[anywhere] * 4 + [vmem] * 3,
+        out_specs=anywhere,
+        scratch_shapes=[
+            pltpu.VMEM((n_sp, model, chunk), bf16),
+            pltpu.VMEM((n_sp, model, chunk), bf16),
+            pltpu.VMEM((n_sp, n_dp, deep, width), bf16),
+            pltpu.VMEM((total, model), bf16),
+            pltpu.VMEM((n_sp, total, chunk), f32),
+            pltpu.VMEM((groups, total, LANES), f32),
+            pltpu.VMEM((groups, round_up(n_taps, 8), LANES), f32),
+            pltpu.VMEM((groups, rows, LANES), bf16),
+            pltpu.VMEM((n_sp, rows, chunk), bf16),
+            pltpu.VMEM((n_dp, rows, width), f32),
+            pltpu.VMEM((n_dp, rows, width), bf16),
+            dma((3, n_sp - 1)),
+            dma((3, n_sp - 1)),
+            dma((3, n_sp)),
+            dma((3, n_sp)),
+            dma((3, n_sp, 2)),
+            dma((3, n_sp, 2)),
+            dma((3, n_sp, 2)),
+            dma((3, n_sp, 2)),
+            dma((2,)),
+            dma((4,)),
+            dma((n_dp,)),
+        ],
+        compiler_params=pltpu.CompilerParams(
+            collective_id=0, has_side_effects=True, vmem_limit_bytes=48 * 2**20
+        ),
+    )(tokens[0], w_value, w_gate, w_out, conv_weight, norm_gain[None], norm_bias[None])
+    return out[None]
 
 
 def passed_along(array, axis, by):
@@ -12,7 +315,7 @@
     return lax.ppermute(array, axis, pairs)
 
 
-def per_device(tokens, w_value, w_gate, conv_weight, norm_gain, norm_bias, w_out):
+def gathered(tokens, w_value, w_gate, conv_weight, norm_gain, norm_bias, w_out):
     pieces = (
         lax.all_gather(w_value, "sp", axis=1, tiled=True),
         lax.all_gather(w_gate, "sp", axis=1, tiled=True),
@@ -50,6 +353,15 @@
     return mixed.astype(jnp.bfloat16)[None]
 
 
+def per_device(sizes, tokens, w_value, w_gate, conv_weight, norm_gain, norm_bias, w_out):
+    args = (tokens, w_value, w_gate, conv_weight, norm_gain, norm_bias, w_out)
+    pair_of_chips = sizes["grp"] == 2 and sizes["dp"] == 4
+    whole_tiles = w_value.shape[1] % LANES == 0 and w_out.shape[1] % LANES == 0
+    if pair_of_chips and whole_tiles and tokens.shape[0] == 1:
+        return fused(sizes["sp"], *args)
+    return gathered(*args)
+
+
 def solution(mesh):
     placed = (
         P(("grp", "dp"), "sp", None),
@@ -61,7 +373,7 @@
         P("sp", "dp"),
     )
     return jax.shard_map(
-        per_device,
+        functools.partial(per_device, dict(mesh.shape)),
         mesh=mesh,
         in_specs=placed,
         out_specs=P(("grp", "dp"), "sp", None),

time: 219 us -> 105 us (0.48)
  waiting for transfers between devices: 177 us -> 0 us
  Pallas kernels: 0 us -> 95.5 us
  matrix products: 18.9 us -> 0 us
  between operations: 13.6 us -> 0.02 us
  starting transfers between devices: 3.3 us -> 0 us
  local copies, waits for them, and re-layouts: 5 us -> 7.61 us
    all_gather x6 -> x0, waiting for transfers between devices: 174 us -> none  [the longest x1 36.1 us: per_device(): lax.all_gather(pieces[1], 'dp', axis=0, tiled=True)]
    pallas_call x0 -> x1, Pallas kernels: none -> 95.5 us  [fused(): pl.pallas_call(functools.partial(fused_kernel, n_sp), out_shape=jax.Shape...]
    dot_general x3 -> x0, matrix products: 15.2 us -> none  [the longest x1 5.51 us: per_device(): mixed = jnp.dot(normed, full_out, preferred_element_type=jnp.float32)]
    unnamed x10 -> x15, local copies, waits for them, and re-layouts: 0.11 us -> 7.61 us
    conv_general_dilated x1 -> x0, matrix products: 3.8 us -> none  [per_device(): lax.conv_general_dilated(extended[None], kernel, (1,), [(0, 0)], dimensio...]
    convert_element_type x2 -> x0, local copies, waits for them, and re-layouts: 3.78 us -> none  [per_device(): conv_f = conv.astype(jnp.float32)]
    ppermute x1 -> x0, starting transfers between devices: 3.11 us -> none  [passed_along(): return lax.ppermute(array, axis, pairs)]
  transfers between devices with their start and end apart: 7 -> 0, of which waited for: 7 -> 0; matrix products, arithmetic and copies ran while one was open for 9% -> 0% of each run, Pallas kernels for 0% -> 0%
where the time goes in v1:
time: 105 us; the launch traced here: 103 us
  Pallas kernels  95.5 us (91%)
  local copies, waits for them, and re-layouts  7.61 us (7%)
    pallas_call x1, Pallas kernels, fused(): pl.pallas_call(functools.partial(fused_kernel, n_sp), out_shape=jax.Shape...  95.5 us
    unnamed x15, local copies, waits for them, and re-layouts  7.61 us

profile of v1, /device:TPU:1, one launch (start us, length us, event | category | flops | bytes accessed | tf_op | source)
XLA Modules:
  0.0 103.1 jit_solution(6795613609265300295)
XLA Ops:
  0.0 0.0 copy-start
  0.0 1.4 %copy-done = bf16[1,384,2048]{2,1,0:T(8,128)(2,1)S(1)} copy-done((bf16[1,384,2048]{2,1,0:T(8,128)(2,1)S(1)}, bf16[1,384,2048]{2,1,0:T(8,128)(2,1)}, u32[]{:S(2)}) %copy-start) | copy-done | bytes 1572888
  1.4 0.0 copy-start.1
  1.4 0.9 copy-done.1
  2.4 0.0 copy-start.2
  2.4 0.9 copy-done.2
  3.3 0.0 copy-start.3
  3.3 0.9 copy-done.3
  4.3 0.0 copy-start.4
  4.3 0.8 copy-done.4
  5.1 0.0 copy-start.5
  5.1 0.7 copy-done.5
  5.8 0.0 copy-start.6
  5.8 0.7 copy-done.6
  6.5 95.5 %shard_map.73 = bf16[384,2048]{1,0:T(8,128)(2,1)S(1)} custom-call(bf16[384,2048]{1,0:T(8,128)(2,1)S(1)} %bitcast.5, bf16[512,256]{1,0:T(8,128)(2,1)S(1)} %copy-done.1, bf16[512,256]{1,0:T(8,128)(2,1)S(1)} %copy-done.2, bf16[256,512]{1,0:T(8,128)(2,1)S(1)} %copy-done.3, bf16[31,1024]{1,0:T(8,128)(2,1)S(1)} %copy-done.4, f32[1,1024]{1,0:T(1,128)S(1)} %bitcast.6, ...), custom_call_target="tpu_custom_call" | custom-call | tf_op jit(solution)/shard_map/pallas_call | solution.py:276
  102.0 1.1 %copy.9 = bf16[1,384,2048]{2,1,0:T(8,128)(2,1)} copy(bf16[1,384,2048]{2,1,0:T(8,128)(2,1)S(1)} %bitcast.4) | data formatting | bytes 3145728
Async XLA Ops:
  0.0 1.4 %copy-start = (bf16[1,384,2048]{2,1,0:T(8,128)(2,1)S(1)}, bf16[1,384,2048]{2,1,0:T(8,128)(2,1)}, u32[]{:S(2)}) copy-start(bf16[1,384,2048]{2,1,0:T(8,128)(2,1)} %param.7) | copy-start | bytes 4718596
  1.4 0.9 copy-start.1
  2.4 0.9 copy-start.2
  3.3 0.9 copy-start.3
  4.3 0.8 copy-start.4
  5.1 0.7 copy-start.5
  5.8 0.7 copy-start.6

commit v2 on v1

--- a/solution.py
+++ b/solution.py
@@ -149,13 +149,16 @@
         part = region(m, at_z(k), dd, start, size)
         send(part, part, y_send.at[m, k, side], y_recv.at[m, k, side], {"grp": 1 - y})
 
-    def step_zx(m, k):
+    def step_z(m, k):
         start, size = share(m)
         if k > 0:
             part = region(m, at_z(k), dp, start, size)
             remote(part, part, z_send.at[m, k - 1], z_recv.at[m, k - 1], {"sp": z}).wait_recv()
             send(part, part, x_send.at[m, k], x_recv.at[m, k], {"dp": across})
             forward_y(m, k, 0, dp)
+
+    def step_x(m, k):
+        start, size = share(m)
         part = region(m, at_z(k), across, start, size)
         remote(part, part, x_send.at[m, k], x_recv.at[m, k], {"dp": across}).wait_recv()
         forward_y(m, k, 1, across)
@@ -246,13 +249,11 @@
                     out_copies.append(copy)
 
     order = [(m, k) for m in range(3) for k in range(n_sp)]
-    for t in range(len(order) + 2):
-        if t < len(order):
-            step_zx(*order[t])
-        if 0 <= t - 1 < len(order):
-            step_y(*order[t - 1])
-        if t >= 2:
-            step_use(*order[t - 2])
+    lags = ((step_z, 0), (step_x, 2), (step_y, 4), (step_use, 5))
+    for t in range(len(order) + lags[-1][1]):
+        for step, lag in lags:
+            if 0 <= t - lag < len(order):
+                step(*order[t - lag])
 
     for copy in started:
         copy.wait_send()
@@ -271,7 +272,7 @@
     total = rows + lead
     bf16, f32 = jnp.bfloat16, jnp.float32
     dma = pltpu.SemaphoreType.DMA
-    anywhere = pl.BlockSpec(memory_space=pl.ANY)
+    anywhere = pl.BlockSpec(memory_space=pltpu.HBM)
     vmem = pl.BlockSpec(memory_space=pltpu.VMEM)
     out = pl.pallas_call(
         functools.partial(fused_kernel, n_sp),
@@ -303,7 +304,7 @@
             dma((n_dp,)),
         ],
         compiler_params=pltpu.CompilerParams(
-            collective_id=0, has_side_effects=True, vmem_limit_bytes=48 * 2**20
+            collective_id=0, has_side_effects=True, vmem_limit_bytes=63 * 2**20
         ),
     )(tokens[0], w_value, w_gate, w_out, conv_weight, norm_gain[None], norm_bias[None])
     return out[None]

time: 105 us -> 80.8 us (0.77); the launches traced: 103 us -> 80.6 us
  Pallas kernels: 95.5 us -> 77.8 us
  local copies, waits for them, and re-layouts: 7.61 us -> 2.73 us
    pallas_call x1, Pallas kernels: 95.5 us -> 77.8 us  [fused(): pl.pallas_call(functools.partial(fused_kernel, n_sp), out_shape=jax.Shape...]
    unnamed x15 -> x1, local copies, waits for them, and re-layouts: 7.61 us -> 2.73 us
where the time goes in v2:
time: 80.8 us; the launch traced here: 80.6 us
  Pallas kernels  77.8 us (96%)
  local copies, waits for them, and re-layouts  2.73 us (3%)
    pallas_call x1, Pallas kernels, fused(): pl.pallas_call(functools.partial(fused_kernel, n_sp), out_shape=jax.Shape...  77.8 us
    unnamed x1, local copies, waits for them, and re-layouts  2.73 us

profile of v2, /device:TPU:1, one launch (start us, length us, event | category | flops | bytes accessed | tf_op | source)
XLA Modules:
  0.0 80.6 jit_solution(1424476523989321186)
XLA Ops:
  0.0 77.8 %shard_map.73 = bf16[384,2048]{1,0:T(8,128)(2,1)} custom-call(bf16[384,2048]{1,0:T(8,128)(2,1)} %bitcast.5, bf16[512,256]{1,0:T(8,128)(2,1)} %wv_ref.1, bf16[512,256]{1,0:T(8,128)(2,1)} %wg_ref.1, bf16[256,512]{1,0:T(8,128)(2,1)} %wo_ref.1, bf16[31,1024]{1,0:T(8,128)(2,1)} %cw_ref.1, f32[1,1024]{1,0:T(1,128)} %bitcast.6, f32[1,1024]{1,0:T(1,128)} %bitcast.7), custom_call_target="tpu_custom_call" | custom-call | tf_op jit(solution)/shard_map/pallas_call | solution.py:277
  77.8 2.7 %copy.9 = bf16[1,384,2048]{2,1,0:T(8,128)(2,1)} copy(bf16[1,384,2048]{2,1,0:T(8,128)(2,1)} %bitcast.4) | data formatting | bytes 3145728

commit v3 on v2

--- a/solution.py
+++ b/solution.py
@@ -71,7 +71,7 @@
 
     def span(m):
         size = own[m].shape[0]
-        only = round_up(size * 5 // 16, PACK)
+        only = round_up(size * (4 if m == 2 else 6) // 16, PACK)
         return size, only, size - only
 
     def region(m, zz, dd, start, size):

time: 80.8 us -> 80.7 us (level)
  no operation moved by 1% of the time
where the time goes in v3:
time: 80.7 us; the launch traced here: 80.4 us
  Pallas kernels  77.7 us (96%)
  local copies, waits for them, and re-layouts  2.73 us (3%)
    pallas_call x1, Pallas kernels, fused(): pl.pallas_call(functools.partial(fused_kernel, n_sp), out_shape=jax.Shape...  77.7 us
    unnamed x1, local copies, waits for them, and re-layouts  2.73 us

profile of v3, /device:TPU:1, one launch (start us, length us, event | category | flops | bytes accessed | tf_op | source)
XLA Modules:
  0.0 80.4 jit_solution(6488131594381074174)
XLA Ops:
  0.0 77.7 %shard_map.73 = bf16[384,2048]{1,0:T(8,128)(2,1)} custom-call(bf16[384,2048]{1,0:T(8,128)(2,1)} %bitcast.5, bf16[512,256]{1,0:T(8,128)(2,1)} %wv_ref.1, bf16[512,256]{1,0:T(8,128)(2,1)} %wg_ref.1, bf16[256,512]{1,0:T(8,128)(2,1)} %wo_ref.1, bf16[31,1024]{1,0:T(8,128)(2,1)} %cw_ref.1, f32[1,1024]{1,0:T(1,128)} %bitcast.6, f32[1,1024]{1,0:T(1,128)} %bitcast.7), custom_call_target="tpu_custom_call" | custom-call | tf_op jit(solution)/shard_map/pallas_call | solution.py:277
  77.7 2.7 %copy.9 = bf16[1,384,2048]{2,1,0:T(8,128)(2,1)} copy(bf16[1,384,2048]{2,1,0:T(8,128)(2,1)} %bitcast.4) | data formatting | bytes 3145728
